TPU v7x, 32 devices: a whole 2x2x4 slice. The times are simulated.
32 devices in a mesh: ep: 8 (over z, y), tp: 4 (over x, core).
Axes of the slice: x: 2, y: 2, z: 4, core: 2. Of those that a mesh axis runs over, the one named last changes fastest.
Arguments:
- queries: bfloat16 [1536, 2048], P('ep', 'tp'), may hold values from -5 to 5
- keys: bfloat16 [1536, 512], P('ep', 'tp'), may hold values from -5 to 5
- values: bfloat16 [1536, 512], P('ep', 'tp'), may hold values from -6 to 6
- query_gain: float32 [128], replicated, may hold values from 0.6 to 6
- key_gain: float32 [128], replicated, may hold values from 0.6 to 6
- out_weight: bfloat16 [2048, 2048], P('tp'), may hold values from -0.125 to 0.125
- mixer_gain: float32 [2048], replicated, may hold values from 0.1 to 1.9
- expert_in: bfloat16 [4096, 2048], P(('ep', 'tp')), may hold values from -6 to 6
- routes: int32 [4096, 2], P(('ep', 'tp')), may hold values from 0 to 7, all different within a row; in each aligned block of 128 rows (0 to 127, 128 to 255, ...) at most 48 rows name the same one
- route_weights: float32 [4096, 2], P(('ep', 'tp')), may hold values from 0.2 to 1
- expert_gain: float32 [2048], replicated, may hold values from 0.5 to 4
- gate_w: bfloat16 [8, 2048, 2048], P('ep', None, 'tp'), may hold values from -0.125 to 0.125
- up_w: bfloat16 [8, 2048, 2048], P('ep', None, 'tp'), may hold values from -0.125 to 0.125
- down_w: bfloat16 [8, 2048, 2048], P('ep', 'tp'), may hold values from -0.125 to 0.125
- ffn_out_gain: float32 [2048], replicated, may hold values from 0.1 to 1.9
Outputs:
- mixer_out: bfloat16 [1536, 2048], P(('ep', 'tp'))
- expert_out: bfloat16 [4096, 2048], P(('ep', 'tp'))
Inputs may be any that keep to these rules, and one draw needn't show every extreme that they name: `routes`: each row names 2 different experts. Among the rows of one device no expert is named by more than 48 rows, and in every draw some expert is named by exactly 48 rows of some device.
All inputs are finite; a program needn't handle non-finite values.
Results may differ from a plain program's by a relative error of at most 0.015.
The roundings to bfloat16 on the way count: a program that leaves them out, or rounds other values in their place, can miss the bound.
Values may be sent and summed in bfloat16 or wider, within the bound.
No kernel may reach another device: no remote copies, remote signals or barrier semaphores. Data moves between devices by JAX's collectives and lax.ppermute only.
A program may use at most 128 MiB of HBM per device.

v0:
```python
import jax
import jax.numpy as jnp
from jax import lax
from jax.sharding import PartitionSpec as P

HEAD = 128
GRID_W = 64
norm_eps = 1e-06
rope_base = 10000.0
clamp_limit = 7.0
sigmoid_slope = 1.702


def rms_scale(values_in, gain):
    return (
        values_in
        * lax.rsqrt(jnp.mean(values_in * values_in, axis=-1, keepdims=True) + norm_eps)
        * gain
    )


def turn_pair(halfpart, cosine, sine):
    first_part, second_part = jnp.split(halfpart, 2, axis=-1)
    return jnp.concatenate(
        [first_part * cosine - second_part * sine, second_part * cosine + first_part * sine],
        axis=-1,
    )


def grid_rotate(field, position):
    half_width = field.shape[-1] // 2
    inverse = rope_base ** (-jnp.arange(0, half_width, 2, dtype=jnp.float32) / half_width)
    grid_row = (position // GRID_W).astype(jnp.float32)
    grid_col = (position % GRID_W).astype(jnp.float32)
    row_angle = (grid_row[:, None] * inverse[None, :])[:, None, :]
    col_angle = (grid_col[:, None] * inverse[None, :])[:, None, :]
    return jnp.concatenate(
        [
            turn_pair(field[..., :half_width], jnp.cos(row_angle), jnp.sin(row_angle)),
            turn_pair(field[..., half_width:], jnp.cos(col_angle), jnp.sin(col_angle)),
        ],
        axis=-1,
    )


def clamped_unit(gate_pre, up_pre):
    gate_cut = jnp.minimum(gate_pre, clamp_limit)
    up_cut = jnp.clip(up_pre, -clamp_limit, clamp_limit)
    return ((up_cut + 1.0) * gate_cut * jax.nn.sigmoid(sigmoid_slope * gate_cut)).astype(
        jnp.bfloat16
    )


def mixer_half(queries, keys, values, query_gain, key_gain, out_weight, mixer_gain):
    local_rows = queries.shape[0]
    kv_local = keys.shape[1] // HEAD
    group_size = queries.shape[1] // HEAD // kv_local
    position = lax.axis_index("ep") * local_rows + jnp.arange(local_rows, dtype=jnp.int32)
    query_f = queries.astype(jnp.float32).reshape(local_rows, kv_local * group_size, HEAD)
    query_norm = grid_rotate(rms_scale(query_f, query_gain), position).astype(jnp.bfloat16)
    query_norm = query_norm.reshape(local_rows, kv_local, group_size, HEAD)
    key_f = keys.astype(jnp.float32).reshape(local_rows, kv_local, HEAD)
    key_norm = grid_rotate(rms_scale(key_f, key_gain), position).astype(jnp.bfloat16)
    key_norm = key_norm.reshape(local_rows, kv_local * HEAD)
    score_scale = HEAD ** (-0.5)
    initial = (
        jnp.full((kv_local, group_size, local_rows), -1e30, jnp.float32),
        jnp.zeros((kv_local, group_size, local_rows), jnp.float32),
        jnp.zeros((kv_local, group_size, local_rows, HEAD), jnp.float32),
    )
    key_piece = lax.all_gather(key_norm, "ep", axis=0, tiled=True)
    value_piece = lax.all_gather(values, "ep", axis=0, tiled=True)
    piece_rows = key_piece.shape[0]
    block_rows = 1
    for candidate in range(min(piece_rows, 1024), 0, -1):
        if piece_rows % candidate == 0:
            block_rows = candidate
            break
    key_blocks = key_piece.reshape(piece_rows // block_rows, block_rows, kv_local, HEAD)
    value_blocks = value_piece.reshape(piece_rows // block_rows, block_rows, kv_local, HEAD)

    def one_block(state, blocks_in):
        running_max, running_total, weighted = state
        key_block, value_block = blocks_in
        scores = (
            jnp.einsum("qhgd,khd->hgqk", query_norm, key_block, preferred_element_type=jnp.float32)
            * score_scale
        )
        new_max = jnp.maximum(running_max, jnp.max(scores, axis=-1))
        factor = jnp.exp(running_max - new_max)
        expo = jnp.exp(scores - new_max[..., None])
        new_total = running_total * factor + jnp.sum(expo, axis=-1)
        new_weighted = weighted * factor[..., None] + jnp.einsum(
            "hgqk,khd->hgqd",
            expo.astype(jnp.bfloat16),
            value_block,
            preferred_element_type=jnp.float32,
        )
        return ((new_max, new_total, new_weighted), None)

    state_out, unused = lax.scan(one_block, initial, (key_blocks, value_blocks))
    final_max, final_total, weighted = state_out
    attended = (weighted / final_total[..., None]).astype(jnp.bfloat16)
    attended = jnp.transpose(attended, (2, 0, 1, 3)).reshape(
        local_rows, kv_local * group_size * HEAD
    )
    share_rows = local_rows // lax.axis_size("tp")
    selected = lax.slice_in_dim(attended, 0, lax.axis_size("tp") * share_rows, axis=0)
    projected = lax.psum_scatter(
        jnp.dot(selected, out_weight, preferred_element_type=jnp.float32).astype(jnp.bfloat16),
        "tp",
        scatter_dimension=0,
        tiled=True,
    ).astype(jnp.float32)
    return rms_scale(projected, mixer_gain).astype(jnp.bfloat16)


def expert_half(expert_in, routes, route_weights, expert_gain, gate_w, up_w, down_w, ffn_out_gain):
    tok_rows = expert_in.shape[0]
    model_width = expert_in.shape[1]
    top_count = routes.shape[1]
    expert_count = lax.axis_size("ep")
    capacity = max(2, (3 * tok_rows * top_count + 2 * expert_count - 1) // (2 * expert_count))
    normed = rms_scale(expert_in.astype(jnp.float32), expert_gain).astype(jnp.bfloat16)
    pair_expert = routes.reshape(-1)
    pair_count = pair_expert.shape[0]
    one_hot = (pair_expert[:, None] == jnp.arange(expert_count, dtype=jnp.int32)[None, :]).astype(
        jnp.int32
    )
    pair_rank = jnp.sum(jnp.cumsum(one_hot, axis=0) * one_hot, axis=1) - 1
    pair_slot = pair_expert * capacity + pair_rank
    slot_pair = (
        jnp.full((expert_count * capacity,), pair_count, jnp.int32)
        .at[pair_slot]
        .set(jnp.arange(pair_count, dtype=jnp.int32))
    )
    padded = jnp.concatenate([normed, jnp.zeros((1, model_width), jnp.bfloat16)], axis=0)
    outgoing = padded[slot_pair // top_count].reshape(expert_count, capacity, model_width)
    gate_local = gate_w[0]
    up_local = up_w[0]
    down_local = down_w[0]
    arrived = lax.all_to_all(outgoing, "ep", split_axis=0, concat_axis=0, tiled=True)
    flat_rows = arrived.reshape(-1, model_width)
    shard_rows = lax.all_gather(flat_rows, "tp", axis=0, tiled=True)
    hidden = clamped_unit(
        jnp.dot(shard_rows, gate_local, preferred_element_type=jnp.float32),
        jnp.dot(shard_rows, up_local, preferred_element_type=jnp.float32),
    )
    selected = lax.slice_in_dim(hidden, 0, lax.axis_size("tp") * flat_rows.shape[0], axis=0)
    result = lax.psum_scatter(
        jnp.dot(selected, down_local, preferred_element_type=jnp.float32).astype(jnp.bfloat16),
        "tp",
        scatter_dimension=0,
        tiled=True,
    )
    finished = result.reshape(arrived.shape)
    returned = lax.all_to_all(finished, "ep", split_axis=0, concat_axis=0, tiled=True)
    pair_result = returned.reshape(-1, model_width)[pair_slot].reshape(
        tok_rows, top_count, model_width
    )
    combined = jnp.einsum("tk,tkd->td", route_weights, pair_result.astype(jnp.float32))
    return rms_scale(combined, ffn_out_gain).astype(jnp.bfloat16)


def local(
    queries,
    keys,
    values,
    query_gain,
    key_gain,
    out_weight,
    mixer_gain,
    expert_in,
    routes,
    route_weights,
    expert_gain,
    gate_w,
    up_w,
    down_w,
    ffn_out_gain,
):
    mixer_out = mixer_half(queries, keys, values, query_gain, key_gain, out_weight, mixer_gain)
    expert_out = expert_half(
        expert_in, routes, route_weights, expert_gain, gate_w, up_w, down_w, ffn_out_gain
    )
    return (mixer_out, expert_out)


def solution(mesh):
    in_specs = (
        P("ep", "tp"),
        P("ep", "tp"),
        P("ep", "tp"),
        P(),
        P(),
        P("tp", None),
        P(),
        P(("ep", "tp"), None),
        P(("ep", "tp"), None),
        P(("ep", "tp"), None),
        P(),
        P("ep", None, "tp"),
        P("ep", None, "tp"),
        P("ep", "tp", None),
        P(),
    )
    out_specs = (P(("ep", "tp"), None), P(("ep", "tp"), None))
    return jax.shard_map(local, mesh=mesh, in_specs=in_specs, out_specs=out_specs, check_vma=False)
```

profile of v0, /device:TPU:0, one launch (start us, length us, event | category | flops | bytes accessed | tf_op | source)
XLA Modules:
  0.0 257.0 jit_solution(10198125140260231767)
XLA Ops:
  7.2 0.9 copy.33
  8.4 0.7 broadcast_multiply_fusion
  10.3 1.4 scatter_custom_fusion
  11.8 1.2 fusion.25
  13.0 1.2 fusion.27
  14.3 3.1 %gather_fusion = bf16[384,2048]{1,0:T(8,128)(2,1)} fusion(bf16[129,2048]{1,0:T(8,128)(2,1)S(1)} %concatenate.47, s32[1024]{0:T(1024)S(1)} %pad_clamp_fusion.1), kind=kCustom, calls=%fused_computation | custom fusion | bytes 3147264 | tf_op jit(solution)/shard_map/gather | solution.py:138
  17.4 44.4 %all_to_all.10 = bf16[8,48,2048]{2,1,0:T(8,128)(2,1)} all-to-all(bf16[8,48,2048]{2,1,0:T(8,128)(2,1)} %bitcast.136), channel_id=1, replica_groups=mesh['ep'=8,'tp'=4] {'ep'}, dimensions={0} | all-to-all | bytes 3145728 | tf_op jit(solution)/shard_map/all_to_all | solution.py:142
  62.1 45.3 %all-gather.2.cloned.1.call-done = bf16[1536,2048]{1,0:T(8,128)(2,1)} async-done(((bf16[384,2048]{1,0:T(8,128)(2,1)}), bf16[1536,2048]{1,0:T(8,128)(2,1)}) %all-gather.2.cloned.1.call-update) | async-done | bytes 6291472 | tf_op jit(solution)/shard_map/all_gather | solution.py:144
  107.4 8.5 %convolution_minimum_fusion = f32[1536,512]{1,0:T(8,128)} fusion(bf16[1536,2048]{1,0:T(8,128)(2,1)} %all-gather.2.cloned.1.call-done, bf16[1,2048,512]{2,1,0:T(8,128)(2,1)} %param.28), kind=kOutput, calls=%fused_computation.30 | convolution fusion | flops 3222011904 | bytes 11534336 | tf_op jit(solution)/shard_map/dot_general | solution.py:146
  115.9 11.9 %convolution_convert_fusion = bf16[1536,2048]{1,0:T(8,128)(2,1)} fusion(bf16[1,512,2048]{2,1,0:T(8,128)(2,1)S(1)} %copy-done, f32[1536,512]{1,0:T(8,128)} %convolution_minimum_fusion, bf16[1536,2048]{1,0:T(8,128)(2,1)} %all-gather.2.cloned.1.call-done, bf16[1,2048,512]{2,1,0:T(8,128)(2,1)} %param.29), kind=kOutput, calls=%fused_computation.28 | convolution fusion | flops 6452674560 | bytes 19922944 | tf_op jit(solution)/shard_map/dot_general | solution.py:151
  127.9 0.9 copy-done.3
  129.3 0.8 multiply_cosine_fusion.1
  130.3 0.7 fusion.38
  131.9 0.8 fusion.63
  132.9 31.2 %all_gather.9 = bf16[1536,128]{1,0:T(8,128)(2,1)S(1)} all-gather(bf16[192,128]{1,0:T(8,128)(2,1)S(1)} %pad_maximum_fusion.1), channel_id=1, replica_groups=mesh['ep'=8,'tp'=4] {'ep'}, dimensions={0}, use_global_device_ids=true | all-gather | bytes 442368 | tf_op jit(solution)/shard_map/all_gather | solution.py:71
  164.1 31.0 %all_gather.10 = bf16[1536,128]{1,0:T(8,128)(2,1)S(1)} all-gather(bf16[192,128]{1,0:T(8,128)(2,1)S(1)} %copy-done.4), channel_id=1, replica_groups=mesh['ep'=8,'tp'=4] {'ep'}, dimensions={0}, use_global_device_ids=true | all-gather | bytes 442368 | tf_op jit(solution)/shard_map/all_gather | solution.py:72
  195.1 10.1 %while.15 = (s32[]{:T(128)}, f32[1,4,192]{2,1,0:T(4,128)S(1)}, f32[1,4,192]{2,1,0:T(4,128)S(1)}, f32[1,4,192,128]{3,2,1,0:T(8,128)S(1)}, bf16[2,768,1,128]{3,1,2...) while((s32[]{:T(128)}, f32[1,4,192]{2,1,0:T(4,128)S(1)}, ...), condition=%wide.region_5.6_spmd.clone, body=%wide.region_2.5_spmd.clone.sunk | while | flops 307008000 | bytes 17942668 | solution.py:101
  195.1 1.9 bitcast_reduce_fusion.2
  197.0 2.5 fusion.94
  199.5 0.6 fusion.93
  200.1 1.9 bitcast_reduce_fusion.2
  202.0 2.5 fusion.94
  204.5 0.6 fusion.93
  205.2 5.6 %all-to-all-start.1 = ((bf16[8,48,2048]{2,1,0:T(8,128)(2,1)}), bf16[8,48,2048]{2,1,0:T(8,128)(2,1)}, u32[]{:S(2)}, u32[]{:S(2)}) async-start(bf16[8,48,2048]{2,1,0:T(8,128)(2,1)} %bitcast.141), calls=%async_computation.3 | async-start | bytes 3145728 | tf_op jit(solution)/shard_map/all_to_all | solution.py:157
  211.4 3.1 %convolution_convert_fusion.1 = bf16[192,2048]{1,0:T(8,128)(2,1)} fusion(bf16[512,2048]{1,0:T(8,128)(2,1)} %param.22, bf16[24,8,4,128]{3,2,1,0:T(4,128)(2,1)S(1)} %bitcast.142), kind=kOutput, calls=%fused_computation.35 | convolution fusion | flops 403046400 | bytes 3080192 | tf_op jit(solution)/shard_map/dot_general | solution.py:110
  214.7 23.4 %reduce-scatter.3.cloned.1.call-done = bf16[48,2048]{1,0:T(8,128)(2,1)} async-done(((bf16[192,2048]{1,0:T(8,128)(2,1)}), bf16[48,2048]{1,0:T(8,128)(2,1)}) %reduce-scatter.3.cloned.1.call-update) | async-done | bytes 196624 | tf_op jit(solution)/shard_map/reduce_scatter | solution.py:109
  238.1 1.1 fusion.33
  239.2 1.7 fusion.35
  240.9 4.0 %gather_fusion.1 = bf16[256,2048]{1,0:T(8,128)(2,1)S(1)} fusion(bf16[384,2048]{1,0:T(8,128)(2,1)} %bitcast.23, s32[1024]{0:T(1024)S(1)} %pad_clamp_fusion), kind=kCustom, calls=%fused_computation.1 | custom fusion | bytes 2098176 | tf_op jit(solution)/shard_map/gather | solution.py:158
  244.9 1.5 reshape.497
  246.4 2.5 fusion.79
  249.3 1.2 fusion.30
  (74 shorter events, 4.8 us)
Async XLA Ops:
  7.2 108.7 %copy-start = (bf16[1,512,2048]{2,1,0:T(8,128)(2,1)S(1)}, bf16[1,512,2048]{2,1,0:T(8,128)(2,1)}, u32[]{:S(2)}) copy-start(bf16[1,512,2048]{2,1,0:T(8,128)(2,1)} %param.30) | copy-start | bytes 6291460
  7.2 100.2 %all-gather.2.cloned.1.call-start = ((), (), s32[]{:S(2)}) async-start(), calls=%async_computation.5 | async-start | bytes 7864320 | tf_op jit(solution)/shard_map/all_gather | solution.py:144
  61.9 143.3 %reduce-scatter.5.cloned.1.call-start = ((), (), s32[]{:S(2)}) async-start(), calls=%async_computation.6 | async-start | bytes 7864320 | tf_op jit(solution)/shard_map/reduce_scatter | solution.py:150
  127.8 0.9 copy-start.3
  127.9 2.2 copy-start.8
  130.0 1.7 copy-start.2
  130.0 1.8 copy-start.9
  130.3 33.7 %copy-start.4 = (bf16[192,128]{1,0:T(8,128)(2,1)S(1)}, bf16[192,128]{1,0:T(8,128)(2,1)}, u32[]{:S(2)}) copy-start(bf16[192,128]{1,0:T(8,128)(2,1)} %param.19) | copy-start | bytes 147460
  197.0 2.5 copy-start.1
  202.0 2.5 copy-start.1
  205.2 35.7 %all-to-all-start.1 = ((bf16[8,48,2048]{2,1,0:T(8,128)(2,1)}), bf16[8,48,2048]{2,1,0:T(8,128)(2,1)}, u32[]{:S(2)}, u32[]{:S(2)}) async-start(bf16[8,48,2048]{2,1,0:T(8,128)(2,1)} %bitcast.141), calls=%async_computation.3 | async-start | bytes 3145728 | tf_op jit(solution)/shard_map/all_to_all | solution.py:157
  210.8 27.3 %reduce-scatter.3.cloned.1.call-start = ((), (), s32[]{:S(2)}) async-start(), calls=%async_computation.4 | async-start | bytes 983040 | tf_op jit(solution)/shard_map/reduce_scatter | solution.py:109
  211.1 3.5 %copy-start.7 = (f32[128,2]{0,1:T(2,128)S(1)}, f32[128,2]{0,1:T(2,128)}, u32[]{:S(2)}) copy-start(f32[128,2]{0,1:T(2,128)} %param.26) | copy-start | bytes 3076
  211.3 27.9 %copy-start.6 = (f32[2048]{0:T(1024)S(1)}, f32[2048]{0:T(1024)}, u32[]{:S(2)}) copy-start(f32[2048]{0:T(1024)} %param.23) | copy-start | bytes 24580
  246.4 2.9 %copy-start.5 = (f32[2048]{0:T(1024)S(1)}, f32[2048]{0:T(1024)}, u32[]{:S(2)}) copy-start(f32[2048]{0:T(1024)} %param.31) | copy-start | bytes 24580
Sparse Core Ops, SparseCore 0:
  62.0 45.3 all-gather.1
  128.0 58.8 reduce-scatter.4
  214.7 23.4 reduce-scatter.2
where the time goes:
time: 258 us; the launch traced here: 257 us
  blocking collectives  107 us (41%)
  waiting for transfers between devices  68.8 us (27%)
  matrix products  34.7 us (13%)
  between operations  14.1 us (5%)
  other arithmetic  13.6 us (5%)
  local copies, waits for them, and re-layouts  13.1 us (5%)
  starting transfers between devices  6.14 us (2%)
    all_gather x1, waiting for transfers between devices, expert_half(): shard_rows = lax.all_gather(flat_rows, 'tp', axis=0, tiled=True)  45.3 us
    all_to_all x1, blocking collectives, expert_half(): lax.all_to_all(outgoing, 'ep', split_axis=0, concat_axis=0, tiled=True)  44.4 us
    all_gather x1, blocking collectives, mixer_half(): key_piece = lax.all_gather(key_norm, 'ep', axis=0, tiled=True)  31.2 us
    all_gather x1, blocking collectives, mixer_half(): value_piece = lax.all_gather(values, 'ep', axis=0, tiled=True)  31 us
    reduce_scatter x1, waiting for transfers between devices, mixer_half(): lax.psum_scatter(jnp.dot(selected, out_weight, preferred_element_type=jnp...  23.4 us
    dot_general x1, matrix products, expert_half(): jnp.dot(selected, down_local, preferred_element_type=jnp.float32)  11.9 us
    dot_general x1, matrix products, expert_half(): jnp.dot(shard_rows, gate_local, preferred_element_type=jnp.float32)  8.52 us
    all_to_all x1, starting transfers between devices, expert_half(): lax.all_to_all(finished, 'ep', split_axis=0, concat_axis=0, tiled=True)  5.62 us
  transfers between devices with their start and end apart: 4, of which 2 were waited for; matrix products, arithmetic and copies ran while one was open for 8% of the time, Pallas kernels for 0%

commit v1 on v0

--- a/solution.py
+++ b/solution.py
@@ -68,8 +68,12 @@
         jnp.zeros((kv_local, group_size, local_rows), jnp.float32),
         jnp.zeros((kv_local, group_size, local_rows, HEAD), jnp.float32),
     )
-    key_piece = lax.all_gather(key_norm, "ep", axis=0, tiled=True)
-    value_piece = lax.all_gather(values, "ep", axis=0, tiled=True)
+    place_state_now = lambda a0, incoming_x, link_axis: jnp.split(
+        lax.all_gather(jnp.concatenate([a0, incoming_x], 1), link_axis, axis=0, tiled=True),
+        [a0.shape[1]],
+        1,
+    )
+    key_piece, value_piece = place_state_now(key_norm, values, "ep")
     piece_rows = key_piece.shape[0]
     block_rows = 1
     for candidate in range(min(piece_rows, 1024), 0, -1):

time: 258 us -> 246 us (0.953)
  blocking collectives: 107 us -> 76.7 us
  waiting for transfers between devices: 68.8 us -> 87 us
    all_gather x2 -> x1, blocking collectives: 62.2 us -> 32.3 us  [mixer_half(): lax.all_gather(jnp.concatenate([a0, incoming_x], 1), link_axis, axis=0, t...]
    reduce_scatter x1, waiting for transfers between devices: 0.02 us -> 11.5 us  [expert_half(): lax.psum_scatter(jnp.dot(selected, down_local, preferred_element_type=jnp...]
    all_to_all x1, waiting for transfers between devices: 0.01 us -> 6.81 us  [expert_half(): lax.all_to_all(finished, 'ep', split_axis=0, concat_axis=0, tiled=True)]
  transfers between devices with their start and end apart: 4 -> 4, of which waited for: 2 -> 4; matrix products, arithmetic and copies ran while one was open for 8% -> 8% of each run, Pallas kernels for 0% -> 0%
where the time goes in v1:
time: 246 us; the launch traced here: 245 us
  waiting for transfers between devices  87 us (35%)
  blocking collectives  76.7 us (31%)
  matrix products  34.7 us (14%)
  between operations  14.1 us (6%)
  other arithmetic  13.4 us (5%)
  local copies, waits for them, and re-layouts  13.3 us (5%)
  starting transfers between devices  6.03 us (2%)
    all_gather x1, waiting for transfers between devices, expert_half(): shard_rows = lax.all_gather(flat_rows, 'tp', axis=0, tiled=True)  45.3 us
    all_to_all x1, blocking collectives, expert_half(): lax.all_to_all(outgoing, 'ep', split_axis=0, concat_axis=0, tiled=True)  44.4 us
    all_gather x1, blocking collectives, mixer_half(): lax.all_gather(jnp.concatenate([a0, incoming_x], 1), link_axis, axis=0, t...  32.3 us
    reduce_scatter x1, waiting for transfers between devices, mixer_half(): lax.psum_scatter(jnp.dot(selected, out_weight, preferred_element_type=jnp...  23.4 us
    dot_general x1, matrix products, expert_half(): jnp.dot(selected, down_local, preferred_element_type=jnp.float32)  11.9 us
    reduce_scatter x1, waiting for transfers between devices, expert_half(): lax.psum_scatter(jnp.dot(selected, down_local, preferred_element_type=jnp...  11.5 us
    dot_general x1, matrix products, expert_half(): jnp.dot(shard_rows, gate_local, preferred_element_type=jnp.float32)  8.52 us
    all_to_all x1, waiting for transfers between devices, expert_half(): lax.all_to_all(finished, 'ep', split_axis=0, concat_axis=0, tiled=True)  6.81 us
  transfers between devices with their start and end apart: 4, of which 4 were waited for; matrix products, arithmetic and copies ran while one was open for 8% of the time, Pallas kernels for 0%

profile of v1, /device:TPU:0, one launch (start us, length us, event | category | flops | bytes accessed | tf_op | source)
XLA Modules:
  0.0 245.4 jit_solution(10976174144972154664)
XLA Ops:
  7.2 0.9 copy.33
  8.4 0.7 broadcast_multiply_fusion
  10.3 1.4 scatter_custom_fusion
  11.8 1.2 fusion.25
  13.0 1.2 fusion.27
  14.3 3.1 %gather_fusion = bf16[384,2048]{1,0:T(8,128)(2,1)} fusion(bf16[129,2048]{1,0:T(8,128)(2,1)S(1)} %concatenate.49, s32[1024]{0:T(1024)S(1)} %pad_clamp_fusion.1), kind=kCustom, calls=%fused_computation | custom fusion | bytes 3147264 | tf_op jit(solution)/shard_map/gather | solution.py:142
  17.4 44.4 %all_to_all.10 = bf16[8,48,2048]{2,1,0:T(8,128)(2,1)} all-to-all(bf16[8,48,2048]{2,1,0:T(8,128)(2,1)} %bitcast.136), channel_id=1, replica_groups=mesh['ep'=8,'tp'=4] {'ep'}, dimensions={0} | all-to-all | bytes 3145728 | tf_op jit(solution)/shard_map/all_to_all | solution.py:146
  62.1 45.3 %all-gather.2.cloned.1.call-done = bf16[1536,2048]{1,0:T(8,128)(2,1)} async-done(((bf16[384,2048]{1,0:T(8,128)(2,1)}), bf16[1536,2048]{1,0:T(8,128)(2,1)}) %all-gather.2.cloned.1.call-update) | async-done | bytes 6291472 | tf_op jit(solution)/shard_map/all_gather | solution.py:148
  107.4 8.5 %convolution_minimum_fusion = f32[1536,512]{1,0:T(8,128)} fusion(bf16[1536,2048]{1,0:T(8,128)(2,1)} %all-gather.2.cloned.1.call-done, bf16[1,2048,512]{2,1,0:T(8,128)(2,1)} %param.28), kind=kOutput, calls=%fused_computation.30 | convolution fusion | flops 3222011904 | bytes 11534336 | tf_op jit(solution)/shard_map/dot_general | solution.py:150
  115.9 11.9 %convolution_convert_fusion = bf16[1536,2048]{1,0:T(8,128)(2,1)} fusion(bf16[1,512,2048]{2,1,0:T(8,128)(2,1)S(1)} %copy-done, f32[1536,512]{1,0:T(8,128)} %convolution_minimum_fusion, bf16[1536,2048]{1,0:T(8,128)(2,1)} %all-gather.2.cloned.1.call-done, bf16[1,2048,512]{2,1,0:T(8,128)(2,1)} %param.29), kind=kOutput, calls=%fused_computation.28 | convolution fusion | flops 6452674560 | bytes 19922944 | tf_op jit(solution)/shard_map/dot_general | solution.py:155
  127.9 0.9 copy-done.3
  129.3 0.8 multiply_cosine_fusion.1
  130.3 0.7 fusion.38
  131.9 0.8 fusion.64
  132.9 32.3 %all_gather.6 = bf16[1536,256]{1,0:T(8,128)(2,1)S(1)} all-gather(bf16[192,256]{1,0:T(8,128)(2,1)S(1)} %concatenate.43), channel_id=1, replica_groups=mesh['ep'=8,'tp'=4] {'ep'}, dimensions={0}, use_global_device_ids=true | all-gather | bytes 884736 | tf_op jit(solution)/shard_map/all_gather | solution.py:72
  165.3 10.1 %while.15 = (s32[]{:T(128)}, f32[1,4,192]{2,1,0:T(4,128)S(1)}, f32[1,4,192]{2,1,0:T(4,128)S(1)}, f32[1,4,192,128]{3,2,1,0:T(8,128)S(1)}, bf16[2,768,1,128]{3,1,2...) while((s32[]{:T(128)}, f32[1,4,192]{2,1,0:T(4,128)S(1)}, ...), condition=%wide.region_5.6_spmd.clone, body=%wide.region_2.5_spmd.clone.sunk | while | flops 307008000 | bytes 17942668 | solution.py:105
  165.3 1.9 bitcast_reduce_fusion.2
  167.2 2.5 %fusion.95 = f32[1,4,192,128]{3,2,1,0:T(8,128)S(1)} fusion(f32[768,192,4]{0,1,2:T(8,128)} %get-tuple-element.176, f32[4,192]{1,0:T(4,128)S(1)} %bitcast.139, f32[1,4,192,128]{3,2,1,0:T(8,128)S(1)} %get-tuple-element.190, bf16[2,768,1,128]{3,1,2,0:T(8,128)(2,1)S(1)} %get-tuple-element.202, s32[]{:T(128)} %get-tuple-element.187, ...), kind=kOutput, calls=%fused_computation.9.clone.1 | convolution fusion | flops 153059328 | bytes 3350533 | tf_op jit(solution)/shard_map/while/body/eval_jaxpr/hgqk,khd->hgqd/dot_general | solution.py:97
  169.7 0.6 fusion.94
  170.4 1.9 bitcast_reduce_fusion.2
  172.3 2.5 %fusion.95 = f32[1,4,192,128]{3,2,1,0:T(8,128)S(1)} fusion(f32[768,192,4]{0,1,2:T(8,128)} %get-tuple-element.176, f32[4,192]{1,0:T(4,128)S(1)} %bitcast.139, f32[1,4,192,128]{3,2,1,0:T(8,128)S(1)} %get-tuple-element.190, bf16[2,768,1,128]{3,1,2,0:T(8,128)(2,1)S(1)} %get-tuple-element.202, s32[]{:T(128)} %get-tuple-element.187, ...), kind=kOutput, calls=%fused_computation.9.clone.1 | convolution fusion | flops 153059328 | bytes 3350533 | tf_op jit(solution)/shard_map/while/body/eval_jaxpr/hgqk,khd->hgqd/dot_general | solution.py:97
  175.4 11.5 %reduce-scatter.5.cloned.1.call-done = bf16[384,2048]{1,0:T(8,128)(2,1)} async-done(((bf16[1536,2048]{1,0:T(8,128)(2,1)}), bf16[384,2048]{1,0:T(8,128)(2,1)}) %reduce-scatter.5.cloned.1.call-update) | async-done | bytes 1572880 | tf_op jit(solution)/shard_map/reduce_scatter | solution.py:154
  186.9 5.5 %all-to-all-start.1 = ((bf16[8,48,2048]{2,1,0:T(8,128)(2,1)}), bf16[8,48,2048]{2,1,0:T(8,128)(2,1)}, u32[]{:S(2)}, u32[]{:S(2)}) async-start(bf16[8,48,2048]{2,1,0:T(8,128)(2,1)} %bitcast.141), calls=%async_computation.3 | async-start | bytes 3145728 | tf_op jit(solution)/shard_map/all_to_all | solution.py:161
  193.0 3.1 %convolution_convert_fusion.1 = bf16[192,2048]{1,0:T(8,128)(2,1)} fusion(bf16[512,2048]{1,0:T(8,128)(2,1)} %param.22, bf16[24,8,4,128]{3,2,1,0:T(4,128)(2,1)S(1)} %bitcast.142), kind=kOutput, calls=%fused_computation.35 | convolution fusion | flops 403046400 | bytes 3080192 | tf_op jit(solution)/shard_map/dot_general | solution.py:114
  196.3 23.4 %reduce-scatter.3.cloned.1.call-done = bf16[48,2048]{1,0:T(8,128)(2,1)} async-done(((bf16[192,2048]{1,0:T(8,128)(2,1)}), bf16[48,2048]{1,0:T(8,128)(2,1)}) %reduce-scatter.3.cloned.1.call-update) | async-done | bytes 196624 | tf_op jit(solution)/shard_map/reduce_scatter | solution.py:113
  219.7 1.1 fusion.33
  220.8 1.7 fusion.35
  222.5 6.8 %all-to-all-done.1 = bf16[8,48,2048]{2,1,0:T(8,128)(2,1)} async-done(((bf16[8,48,2048]{2,1,0:T(8,128)(2,1)}), bf16[8,48,2048]{2,1,0:T(8,128)(2,1)}, u32[]{:S(2)}, u32[]{:S(2)}) %all-to-all-start.1) | async-done | bytes 1572896 | tf_op jit(solution)/shard_map/all_to_all | solution.py:161
  229.3 4.0 %gather_fusion.1 = bf16[256,2048]{1,0:T(8,128)(2,1)S(1)} fusion(bf16[384,2048]{1,0:T(8,128)(2,1)} %bitcast.23, s32[1024]{0:T(1024)S(1)} %pad_clamp_fusion), kind=kCustom, calls=%fused_computation.1 | custom fusion | bytes 2098176 | tf_op jit(solution)/shard_map/gather | solution.py:162
  233.3 1.5 reshape.497
  234.8 2.5 %fusion.80 = f32[128,1,2048]{2,1,0:T(1,128)S(1)} fusion(bf16[128,2,2048]{2,1,0:T(2,128)(2,1)} %reshape.497, bf16[128,2,1]{1,2,0:T(2,128)(2,1)S(1)} %copy.35), kind=kOutput, calls=%fused_computation.144 | convolution fusion | flops 1048576 | bytes 2097664 | tf_op jit(solution)/shard_map/tk,tkd->td/dot_general | solution.py:165
  237.7 1.2 fusion.30
  (74 shorter events, 5.5 us)
Async XLA Ops:
  7.2 108.7 %copy-start = (bf16[1,512,2048]{2,1,0:T(8,128)(2,1)S(1)}, bf16[1,512,2048]{2,1,0:T(8,128)(2,1)}, u32[]{:S(2)}) copy-start(bf16[1,512,2048]{2,1,0:T(8,128)(2,1)} %param.30) | copy-start | bytes 6291460
  7.2 100.2 %all-gather.2.cloned.1.call-start = ((), (), s32[]{:S(2)}) async-start(), calls=%async_computation.5 | async-start | bytes 7864320 | tf_op jit(solution)/shard_map/all_gather | solution.py:148
  61.9 125.0 %reduce-scatter.5.cloned.1.call-start = ((), (), s32[]{:S(2)}) async-start(), calls=%async_computation.6 | async-start | bytes 7864320 | tf_op jit(solution)/shard_map/reduce_scatter | solution.py:154
  127.8 0.9 copy-start.3
  127.9 2.2 copy-start.8
  130.0 1.7 copy-start.2
  130.0 1.8 copy-start.9
  130.3 2.5 %copy-start.4 = (bf16[192,128]{1,0:T(8,128)(2,1)S(1)}, bf16[192,128]{1,0:T(8,128)(2,1)}, u32[]{:S(2)}) copy-start(bf16[192,128]{1,0:T(8,128)(2,1)} %param.19) | copy-start | bytes 147460
  167.2 2.5 %copy-start.1 = (f32[768,192,4]{0,1,2:T(8,128)S(1)}, f32[768,192,4]{0,1,2:T(8,128)}, u32[]{:S(2)}) copy-start(f32[768,192,4]{0,1,2:T(8,128)} %get-tuple-element.176) | copy-start | bytes 7077892 | tf_op jit(solution)/shard_map/while
  172.3 2.5 %copy-start.1 = (f32[768,192,4]{0,1,2:T(8,128)S(1)}, f32[768,192,4]{0,1,2:T(8,128)}, u32[]{:S(2)}) copy-start(f32[768,192,4]{0,1,2:T(8,128)} %get-tuple-element.176) | copy-start | bytes 7077892 | tf_op jit(solution)/shard_map/while
  186.9 42.5 %all-to-all-start.1 = ((bf16[8,48,2048]{2,1,0:T(8,128)(2,1)}), bf16[8,48,2048]{2,1,0:T(8,128)(2,1)}, u32[]{:S(2)}, u32[]{:S(2)}) async-start(bf16[8,48,2048]{2,1,0:T(8,128)(2,1)} %bitcast.141), calls=%async_computation.3 | async-start | bytes 3145728 | tf_op jit(solution)/shard_map/all_to_all | solution.py:161
  192.4 27.3 %reduce-scatter.3.cloned.1.call-start = ((), (), s32[]{:S(2)}) async-start(), calls=%async_computation.4 | async-start | bytes 983040 | tf_op jit(solution)/shard_map/reduce_scatter | solution.py:113
  192.7 3.5 %copy-start.7 = (f32[128,2]{0,1:T(2,128)S(1)}, f32[128,2]{0,1:T(2,128)}, u32[]{:S(2)}) copy-start(f32[128,2]{0,1:T(2,128)} %param.26) | copy-start | bytes 3076
  192.9 28.0 %copy-start.6 = (f32[2048]{0:T(1024)S(1)}, f32[2048]{0:T(1024)}, u32[]{:S(2)}) copy-start(f32[2048]{0:T(1024)} %param.23) | copy-start | bytes 24580
  234.8 2.9 %copy-start.5 = (f32[2048]{0:T(1024)S(1)}, f32[2048]{0:T(1024)}, u32[]{:S(2)}) copy-start(f32[2048]{0:T(1024)} %param.31) | copy-start | bytes 24580
Sparse Core Ops, SparseCore 0:
  62.0 45.3 all-gather.1
  128.0 58.8 reduce-scatter.4
  196.2 23.4 reduce-scatter.2
